TPU v7x, 32 devices: a whole 2x2x4 slice. The times are simulated.
32 devices in a mesh: kv: 4 (over y, x), tp: 8 (over z, core).
Axes of the slice: x: 2, y: 2, z: 4, core: 2. Of those that a mesh axis runs over, the one named last changes fastest.
Arguments:
- residual: bfloat16 [128, 4096], P(None, ('kv', 'tp')), may hold values from -20 to 20
- mixer_gain: float32 [4096], P('kv'), may hold values from 0.1 to 1.9
- w_query: bfloat16 [4096, 4096], P('kv', 'tp'), may hold values from -0.09375 to 0.09375
- w_forget: bfloat16 [4096, 4096], P('kv', 'tp'), may hold values from -0.09375 to 0.09375
- w_input: bfloat16 [4096, 4096], P('kv', 'tp'), may hold values from -0.09375 to 0.09375
- w_outgate: bfloat16 [4096, 4096], P('kv', 'tp'), may hold values from -0.09375 to 0.09375
- lower_bound: float32 [4096], P('tp'), may hold values from 0.3 to 0.97
- state: float32 [128, 32, 128, 128], P('kv', 'tp'), may hold values from -6 to 6
- head_gain: float32 [128], replicated, may hold values from 0.1 to 1.9
- w_mix_out: bfloat16 [4096, 4096], P('tp', 'kv'), may hold values from -0.09375 to 0.09375
- ffn_gain: float32 [4096], P('kv'), may hold values from 0.1 to 1.9
- w_gate: bfloat16 [4096, 10752], P('kv', 'tp'), may hold values from -0.09375 to 0.09375
- w_up: bfloat16 [4096, 10752], P('kv', 'tp'), may hold values from -0.09375 to 0.09375
- w_down: bfloat16 [10752, 4096], P('tp', 'kv'), may hold values from -0.0625 to 0.0625
Outputs:
- layer_out: bfloat16 [128, 4096], P(None, ('kv', 'tp'))
- new_state: float32 [128, 32, 128, 128], P('kv', 'tp')
All inputs are finite; a program needn't handle non-finite values.
Results may differ from a plain program's by a relative error of at most 0.015.
Values may be sent and summed in bfloat16 or wider, within the bound.
No kernel may reach another device: no remote copies, remote signals or barrier semaphores. Data moves between devices by JAX's collectives and lax.ppermute only.
A program may use at most 64 MiB of HBM per device.

v0:
```python
import jax
import jax.numpy as jnp
from jax import lax
from jax.sharding import PartitionSpec as P

D = 4096
DK = 128
DV = 128
EPS = 1e-06


def project_row(weight, piece):
    return jnp.dot(piece, weight, preferred_element_type=jnp.float32)


def channel_mix(rows_in, ffn_gain, w_gate, w_up, w_down):
    rows_float = rows_in.astype(jnp.float32)
    squares = jnp.sum(rows_float * rows_float, axis=1)
    scaled = (rows_float * ffn_gain).astype(jnp.bfloat16)
    gate = jnp.dot(scaled, w_gate, preferred_element_type=jnp.float32)
    upper = jnp.dot(scaled, w_up, preferred_element_type=jnp.float32)
    whole_total = lax.psum(squares, "kv")
    gate, upper = (
        lax.psum(gate.astype(jnp.bfloat16), "kv").astype(jnp.float32),
        lax.psum(upper.astype(jnp.bfloat16), "kv").astype(jnp.float32),
    )
    inverse = lax.rsqrt(whole_total / D + EPS)[:, None]
    hidden = (jax.nn.silu(gate * inverse) * (upper * inverse)).astype(jnp.bfloat16)
    terms = jnp.dot(hidden, w_down, preferred_element_type=jnp.float32)
    summed = lax.psum_scatter(
        terms.astype(jnp.bfloat16), "tp", scatter_dimension=1, tiled=True
    ).astype(jnp.float32)
    width = summed.shape[1]
    own = lax.dynamic_slice_in_dim(rows_float, lax.axis_index("tp") * width, width, 1)
    return (own + summed).astype(jnp.bfloat16)


def body(
    residual,
    mixer_gain,
    w_query,
    w_forget,
    w_input,
    w_outgate,
    lower_bound,
    state,
    head_gain,
    w_mix_out,
    ffn_gain,
    w_gate,
    w_up,
    w_down,
):
    local_seqs, local_heads = (state.shape[0], state.shape[1])
    rows = lax.all_gather(residual, "tp", axis=1, tiled=True)
    rows_float = rows.astype(jnp.float32)
    squares = jnp.sum(rows_float * rows_float, axis=1)
    scaled = (rows_float * mixer_gain).astype(jnp.bfloat16)
    part_query = jnp.dot(scaled, w_query, preferred_element_type=jnp.float32)
    part_forget = jnp.dot(scaled, w_forget, preferred_element_type=jnp.float32)
    part_value = jnp.dot(scaled, w_input, preferred_element_type=jnp.float32)
    part_gate = jnp.dot(scaled, w_outgate, preferred_element_type=jnp.float32)
    whole_total = lax.psum(squares, "kv")
    total = lax.dynamic_slice_in_dim(whole_total, lax.axis_index("kv") * local_seqs, local_seqs)
    part_query, part_forget, part_value, part_gate = (
        lax.psum_scatter(part_query, "kv", scatter_dimension=0, tiled=True),
        lax.psum_scatter(part_forget, "kv", scatter_dimension=0, tiled=True),
        lax.psum_scatter(part_value, "kv", scatter_dimension=0, tiled=True),
        lax.psum_scatter(part_gate, "kv", scatter_dimension=0, tiled=True),
    )
    inverse = lax.rsqrt(total / D + EPS)[:, None]
    bound = lower_bound.reshape(local_heads, DK)
    forget_raw = (part_forget * inverse).reshape(local_seqs, local_heads, DK)
    forget = bound + (1.0 - bound) * jax.nn.sigmoid(forget_raw)
    keyvec = (1.0 - bound) * jax.nn.sigmoid(-forget_raw)
    query = jax.nn.silu((part_query * inverse).reshape(local_seqs, local_heads, DK))
    values = (part_value * inverse).reshape(local_seqs, local_heads, DV)
    updated = forget[..., None] * state + keyvec[..., None] * values[:, :, None, :]
    head_out = jnp.einsum("shc,shce->she", query, updated, precision=lax.Precision.HIGHEST)
    inv_head = lax.rsqrt(jnp.mean(head_out * head_out, axis=2, keepdims=True) + EPS)
    out_gate = jax.nn.silu((part_gate * inverse).reshape(local_seqs, local_heads, DV))
    normed = (
        (head_out * inv_head * head_gain * out_gate)
        .reshape(local_seqs, local_heads * DV)
        .astype(jnp.bfloat16)
    )
    terms = project_row(w_mix_out, lax.all_gather(normed, "kv", axis=0, tiled=True))
    mixed = lax.psum(terms, "tp")
    after_mix = (rows_float + mixed).astype(jnp.bfloat16)
    layer_out = channel_mix(after_mix, ffn_gain, w_gate, w_up, w_down)
    return (layer_out, updated)


def solution(mesh):
    in_specs = (
        P(None, ("kv", "tp")),
        P("kv"),
        P("kv", "tp"),
        P("kv", "tp"),
        P("kv", "tp"),
        P("kv", "tp"),
        P("tp"),
        P("kv", "tp", None, None),
        P(),
        P("tp", "kv"),
        P("kv"),
        P("kv", "tp"),
        P("kv", "tp"),
        P("tp", "kv"),
    )
    out_specs = (P(None, ("kv", "tp")), P("kv", "tp", None, None))
    return jax.shard_map(body, mesh=mesh, in_specs=in_specs, out_specs=out_specs, check_vma=False)
```

profile of v0, /device:TPU:0, one launch (start us, length us, event | category | flops | bytes accessed | tf_op | source)
XLA Modules:
  0.0 312.9 jit_solution(12020792351462122957)
XLA Ops:
  7.2 15.1 %all_gather.6 = bf16[128,1024]{1,0:T(8,128)(2,1)S(1)} all-gather(bf16[128,128]{1,0:T(8,128)(2,1)} %param.14), channel_id=1, replica_groups=mesh['kv'=4,'tp'=8] {'tp'}, dimensions={1}, use_global_device_ids=true | all-gather | bytes 294912 | tf_op jit(solution)/shard_map/all_gather | solution.py:55
  22.4 2.3 fusion.10
  24.7 2.2 fusion.8
  27.0 2.3 fusion.6
  29.4 2.3 fusion.12
  31.8 9.9 %psum.35 = f32[128]{0:T(128)S(1)} all-reduce(f32[128]{0:T(128)S(1)} %fusion.1), channel_id=1, replica_groups=mesh['kv'=4,'tp'=8] {'kv'}, use_global_device_ids=true, to_apply=%region_2.0 | all-reduce | flops 128 | bytes 1024 | tf_op jit(solution)/shard_map/psum | solution.py:63
  42.5 6.5 %reduce-scatter.10.cloned.1.call-done = f32[32,512]{1,0:T(8,128)} async-done(((f32[128,512]{1,0:T(8,128)}), f32[32,512]{1,0:T(8,128)}) %reduce-scatter.10.cloned.1.call-update) | async-done | bytes 65552 | tf_op jit(solution)/shard_map/reduce_scatter | solution.py:67
  49.0 27.1 %reduce-scatter.12.cloned.1.call-done = f32[32,512]{1,0:T(8,128)} async-done(((f32[128,512]{1,0:T(8,128)}), f32[32,512]{1,0:T(8,128)}) %reduce-scatter.12.cloned.1.call-update) | async-done | bytes 65552 | tf_op jit(solution)/shard_map/reduce_scatter | solution.py:68
  76.1 27.2 %reduce-scatter.14.cloned.1.call-done = f32[32,512]{1,0:T(8,128)} async-done(((f32[128,512]{1,0:T(8,128)}), f32[32,512]{1,0:T(8,128)}) %reduce-scatter.14.cloned.1.call-update) | async-done | bytes 65552 | tf_op jit(solution)/shard_map/reduce_scatter | solution.py:69
  103.3 27.0 %reduce-scatter.8.cloned.1.call-done = f32[32,512]{1,0:T(8,128)} async-done(((f32[128,512]{1,0:T(8,128)}), f32[32,512]{1,0:T(8,128)}) %reduce-scatter.8.cloned.1.call-update) | async-done | bytes 65552 | tf_op jit(solution)/shard_map/reduce_scatter | solution.py:66
  130.3 1.0 add_divide_fusion.1
  131.6 8.2 %multiply_add_fusion = f32[32,4,128,128]{3,2,1,0:T(8,128)S(1)} fusion(f32[32,4,128,128]{3,2,1,0:T(8,128)} %param.21, f32[32,4,128]{2,1,0:T(4,128)S(1)} %mul.164, f32[32,4,128]{2,1,0:T(4,128)S(1)} %bitcast.35, f32[32,4,128]{2,1,0:T(4,128)S(1)} %bitcast.34), kind=kLoop, calls=%fused_computation | loop fusion | flops 6291456 | bytes 16973824 | tf_op jit(solution)/shard_map/add | solution.py:78
  139.9 3.4 %copy-done.1 = f32[32,4,128,128]{3,2,1,0:T(8,128)} copy-done((f32[32,4,128,128]{3,2,1,0:T(8,128)}, f32[32,4,128,128]{3,2,1,0:T(8,128)S(1)}, u32[]{:S(2)}) %copy-start.1) | copy-done | bytes 8388632
  143.2 7.2 %fusion.18 = f32[32,4,1,128]{3,2,1,0:T(1,128)S(1)} fusion(f32[32,4,128,1]{2,3,1,0:T(1,128)S(1)} %bitcast.33, f32[32,4,128,128]{3,2,1,0:T(8,128)S(1)} %multiply_add_fusion), kind=kOutput, calls=%fused_computation.39 | convolution fusion | flops 25165824 | bytes 8519680 | tf_op jit(solution)/shard_map/shc,shce->she/dot_general | solution.py:79
  150.8 8.5 %all_gather.7 = bf16[128,512]{1,0:T(8,128)(2,1)S(1)} all-gather(bf16[32,512]{1,0:T(8,128)(2,1)S(1)} %bitcast.38), channel_id=1, replica_groups=mesh['kv'=4,'tp'=8] {'kv'}, dimensions={0}, use_global_device_ids=true | all-gather | bytes 163840 | tf_op jit(solution)/shard_map/all_gather | solution.py:87
  159.2 1.1 fusion.19
  160.4 56.7 %all-reduce.4.cloned.1.call-done = f32[128,1024]{1,0:T(8,128)} async-done(((f32[128,1024]{1,0:T(8,128)}), f32[128,1024]{1,0:T(8,128)}) %all-reduce.4.cloned.1.call-update) | async-done | bytes 524304 | tf_op jit(solution)/shard_map/psum | solution.py:88
  217.1 1.2 multiply_reduce_fusion
  218.3 1.6 convolution_convert_fusion
  219.9 3.4 %convolution_convert_fusion.1 = bf16[128,1344]{0,1:T(8,128)(2,1)} fusion(bf16[1024,1344]{0,1:T(8,128)(2,1)} %param.25, f32[128,1024]{1,0:T(8,128)S(1)} %get-tuple-element.5, f32[1024]{0:T(1024)S(1)} %copy-done.3), kind=kOutput, calls=%fused_computation.2 | convolution fusion | flops 352755712 | bytes 3624960 | tf_op jit(solution)/shard_map/dot_general | solution.py:20
  223.4 10.2 %psum.38 = f32[128]{0:T(128)S(1)} all-reduce(f32[128]{0:T(128)S(1)} %get-tuple-element.4), channel_id=1, replica_groups=mesh['kv'=4,'tp'=8] {'kv'}, use_global_device_ids=true, to_apply=%region_10.11 | all-reduce | flops 128 | bytes 1024 | tf_op jit(solution)/shard_map/psum | solution.py:22
  233.6 36.4 %all-reduce.6.cloned.1.call-done = (bf16[128,1344]{0,1:T(8,128)(2,1)}, bf16[128,1344]{0,1:T(8,128)(2,1)}) async-done(((bf16[128,1344]{0,1:T(8,128)(2,1)}, bf16[128,1344]{0,1:T(8,128)(2,1)}), (bf16[128,1344]{0,1:T(8,128)(2,1)}, bf16[128,1344]{0,1:T(8,128)(2,1)})) %all-reduce.6.cloned.1.call-update) | async-done | bytes 688144 | tf_op jit(solution)/shard_map/psum | solution.py:25
  270.0 2.8 convolution_convert_fusion.2
  273.6 31.0 %reduce-scatter.16.cloned.1.call-done = bf16[128,128]{1,0:T(8,128)(2,1)} async-done(((bf16[1024,128]{1,0:T(8,128)(2,1)}), bf16[128,128]{1,0:T(8,128)(2,1)}) %reduce-scatter.16.cloned.1.call-update) | async-done | bytes 32784
  (45 shorter events, 4.1 us)
Async XLA Ops:
  7.2 211.1 %copy-start = (bf16[1024,1344]{0,1:T(8,128)(2,1)S(1)}, bf16[1024,1344]{0,1:T(8,128)(2,1)}, u32[]{:S(2)}) copy-start(bf16[1024,1344]{0,1:T(8,128)(2,1)} %param.26) | copy-start | bytes 8257540
  7.2 124.4 %copy-start.4 = (f32[512]{0:T(512)S(1)}, f32[512]{0:T(512)}, u32[]{:S(2)}) copy-start(f32[512]{0:T(512)} %param.20) | copy-start | bytes 6148
  7.2 41.8 %reduce-scatter.10.cloned.1.call-start = ((), (), s32[]{:S(2)}) async-start(), calls=%async_computation.6 | async-start | bytes 327680 | tf_op jit(solution)/shard_map/reduce_scatter | solution.py:67
  24.7 51.5 %reduce-scatter.12.cloned.1.call-start = ((), (), s32[]{:S(2)}) async-start(), calls=%async_computation.7 | async-start | bytes 327680 | tf_op jit(solution)/shard_map/reduce_scatter | solution.py:68
  27.0 76.3 %reduce-scatter.14.cloned.1.call-start = ((), (), s32[]{:S(2)}) async-start(), calls=%async_computation.8 | async-start | bytes 327680 | tf_op jit(solution)/shard_map/reduce_scatter | solution.py:69
  29.3 101.0 %reduce-scatter.8.cloned.1.call-start = ((), (), s32[]{:S(2)}) async-start(), calls=%async_computation.5 | async-start | bytes 327680 | tf_op jit(solution)/shard_map/reduce_scatter | solution.py:66
  31.7 185.4 %all-reduce.4.cloned.1.call-start = ((), (), s32[]{:S(2)}) async-start(), calls=%async_computation.9 | async-start | bytes 1048576 | tf_op jit(solution)/shard_map/psum | solution.py:88
  139.8 3.4 %copy-start.1 = (f32[32,4,128,128]{3,2,1,0:T(8,128)}, f32[32,4,128,128]{3,2,1,0:T(8,128)S(1)}, u32[]{:S(2)}) copy-start(f32[32,4,128,128]{3,2,1,0:T(8,128)S(1)} %multiply_add_fusion) | copy-start | bytes 25165828
  139.8 10.8 %copy-start.5 = (f32[128]{0:T(128)S(1)}, f32[128]{0:T(128)}, u32[]{:S(2)}) copy-start(f32[128]{0:T(128)} %param.22) | copy-start | bytes 1540
  139.9 19.4 %copy-start.2 = (bf16[512,1024]{1,0:T(8,128)(2,1)S(1)}, bf16[512,1024]{1,0:T(8,128)(2,1)}, u32[]{:S(2)}) copy-start(bf16[512,1024]{1,0:T(8,128)(2,1)} %param.23) | copy-start | bytes 3145732
  139.9 78.4 %copy-start.3 = (f32[1024]{0:T(1024)S(1)}, f32[1024]{0:T(1024)}, u32[]{:S(2)}) copy-start(f32[1024]{0:T(1024)} %param.24) | copy-start | bytes 12292
  160.4 109.6 %all-reduce.6.cloned.1.call-start = ((), (), s32[]{:S(2)}) async-start(), calls=%async_computation.11 | async-start | bytes 1376256 | tf_op jit(solution)/shard_map/psum | solution.py:25
  223.4 81.2 %reduce-scatter.16.cloned.1.call-start = ((), (), s32[]{:S(2)}) async-start(), calls=%async_computation.10 | async-start | bytes 294912
Sparse Core Ops, SparseCore 0:
  24.8 24.1 reduce-scatter.9
  51.7 24.3 reduce-scatter.11
  78.9 24.3 reduce-scatter.13
  105.9 24.3 reduce-scatter.7
  160.5 56.5 all-reduce.3
  223.5 46.4 all-reduce.5
  273.7 30.7 reduce-scatter.15
where the time goes:
time: 314 us; the launch traced here: 313 us
  waiting for transfers between devices  212 us (68%)
  blocking collectives  43.7 us (14%)
  matrix products  25.2 us (8%)
  between operations  14.3 us (5%)
  other arithmetic  12.3 us (4%)
  local copies, waits for them, and re-layouts  5.22 us (2%)
    psum x1, waiting for transfers between devices, body(): mixed = lax.psum(terms, 'tp')  56.7 us
    psum x1, waiting for transfers between devices, channel_mix(): lax.psum(upper.astype(jnp.bfloat16), 'kv').astype(jnp.float32)  36.4 us
    unnamed x8, waiting for transfers between devices  31.1 us
    reduce_scatter x1, waiting for transfers between devices, body(): lax.psum_scatter(part_gate, 'kv', scatter_dimension=0, tiled=True)  27.2 us
    reduce_scatter x1, waiting for transfers between devices, body(): lax.psum_scatter(part_value, 'kv', scatter_dimension=0, tiled=True)  27.1 us
    reduce_scatter x1, waiting for transfers between devices, body(): lax.psum_scatter(part_query, 'kv', scatter_dimension=0, tiled=True)  27 us
    all_gather x1, blocking collectives, body(): rows = lax.all_gather(residual, 'tp', axis=1, tiled=True)  15.1 us
    psum x1, blocking collectives, channel_mix(): whole_total = lax.psum(squares, 'kv')  10.2 us
  transfers between devices with their start and end apart: 7, of which 7 were waited for; matrix products, arithmetic and copies ran while one was open for 2% of the time, Pallas kernels for 0%

commit v1 on v0

--- a/solution.py
+++ b/solution.py
@@ -14,6 +14,10 @@
 
 
 def channel_mix(rows_in, ffn_gain, w_gate, w_up, w_down):
+
+    def bind_values_up(buf, along_axis):
+        return jnp.sum(lax.all_gather(buf, along_axis), axis=0)
+
     rows_float = rows_in.astype(jnp.float32)
     squares = jnp.sum(rows_float * rows_float, axis=1)
     scaled = (rows_float * ffn_gain).astype(jnp.bfloat16)
@@ -22,7 +26,7 @@
     whole_total = lax.psum(squares, "kv")
     gate, upper = (
         lax.psum(gate.astype(jnp.bfloat16), "kv").astype(jnp.float32),
-        lax.psum(upper.astype(jnp.bfloat16), "kv").astype(jnp.float32),
+        bind_values_up(upper.astype(jnp.bfloat16), "kv").astype(jnp.float32),
     )
     inverse = lax.rsqrt(whole_total / D + EPS)[:, None]
     hidden = (jax.nn.silu(gate * inverse) * (upper * inverse)).astype(jnp.bfloat16)

time: 314 us -> 335 us (1.067)
  waiting for transfers between devices: 212 us -> 225 us
  other arithmetic: 12.3 us -> 20.6 us
    all_gather x0 -> x1, waiting for transfers between devices: none -> 14.4 us  [bind_values_up(): return jnp.sum(lax.all_gather(buf, along_axis), axis=0)]
    reduce_sum x0 -> x1, other arithmetic: none -> 8.94 us  [bind_values_up(): return jnp.sum(lax.all_gather(buf, along_axis), axis=0)]
    all_gather x0 -> x1, local copies, waits for them, and re-layouts: none -> 3.66 us  [bind_values_up(): return jnp.sum(lax.all_gather(buf, along_axis), axis=0)]
    unnamed x8 -> x9, waiting for transfers between devices: 31.1 us -> 31.2 us
  transfers between devices with their start and end apart: 7 -> 8, of which waited for: 7 -> 8; matrix products, arithmetic and copies ran while one was open for 2% -> 7% of each run, Pallas kernels for 0% -> 0%
where the time goes in v1:
time: 335 us
  waiting for transfers between devices  225 us (67%)
  blocking collectives  43.9 us (13%)
  matrix products  25.2 us (8%)
  other arithmetic  20.6 us (6%)
  between operations  14.4 us (4%)
  local copies, waits for them, and re-layouts  5.53 us (2%)
    psum x1, waiting for transfers between devices, body(): mixed = lax.psum(terms, 'tp')  56.6 us
    psum x1, waiting for transfers between devices, channel_mix(): lax.psum(gate.astype(jnp.bfloat16), 'kv').astype(jnp.float32)  34.2 us
    unnamed x9, waiting for transfers between devices  31.2 us
    reduce_scatter x1, waiting for transfers between devices, body(): lax.psum_scatter(part_gate, 'kv', scatter_dimension=0, tiled=True)  27.1 us
    reduce_scatter x1, waiting for transfers between devices, body(): lax.psum_scatter(part_value, 'kv', scatter_dimension=0, tiled=True)  27.1 us
    reduce_scatter x1, waiting for transfers between devices, body(): lax.psum_scatter(part_query, 'kv', scatter_dimension=0, tiled=True)  27 us
    all_gather x1, blocking collectives, body(): rows = lax.all_gather(residual, 'tp', axis=1, tiled=True)  15.1 us
    all_gather x1, waiting for transfers between devices, bind_values_up(): return jnp.sum(lax.all_gather(buf, along_axis), axis=0)  14.4 us
  transfers between devices with their start and end apart: 8, of which 8 were waited for; matrix products, arithmetic and copies ran while one was open for 7% of the time, Pallas kernels for 0%

profile of v1, /device:TPU:0, one launch (start us, length us, event | category | flops | bytes accessed | tf_op | source)
XLA Modules:
  0.0 334.5 jit_solution(1589188580385244822)
XLA Ops:
  7.2 15.1 %all_gather.12 = bf16[128,1024]{1,0:T(8,128)(2,1)S(1)} all-gather(bf16[128,128]{1,0:T(8,128)(2,1)} %param.14), channel_id=1, replica_groups=mesh['kv'=4,'tp'=8] {'tp'}, dimensions={1}, use_global_device_ids=true | all-gather | bytes 294912 | tf_op jit(solution)/shard_map/all_gather | solution.py:59
  22.4 2.3 fusion.10
  24.7 2.2 fusion.8
  27.1 2.2 fusion.6
  29.4 2.2 fusion.12
  31.8 9.9 %psum.28 = f32[128]{0:T(128)S(1)} all-reduce(f32[128]{0:T(128)S(1)} %fusion.1), channel_id=1, replica_groups=mesh['kv'=4,'tp'=8] {'kv'}, use_global_device_ids=true, to_apply=%region_2.0 | all-reduce | flops 128 | bytes 1024 | tf_op jit(solution)/shard_map/psum | solution.py:67
  41.8 7.1 %reduce-scatter.10.cloned.1.call-done = f32[32,512]{1,0:T(8,128)} async-done(((f32[128,512]{1,0:T(8,128)}), f32[32,512]{1,0:T(8,128)}) %reduce-scatter.10.cloned.1.call-update) | async-done | bytes 65552 | tf_op jit(solution)/shard_map/reduce_scatter | solution.py:71
  49.0 27.1 %reduce-scatter.12.cloned.1.call-done = f32[32,512]{1,0:T(8,128)} async-done(((f32[128,512]{1,0:T(8,128)}), f32[32,512]{1,0:T(8,128)}) %reduce-scatter.12.cloned.1.call-update) | async-done | bytes 65552 | tf_op jit(solution)/shard_map/reduce_scatter | solution.py:72
  76.1 27.1 %reduce-scatter.14.cloned.1.call-done = f32[32,512]{1,0:T(8,128)} async-done(((f32[128,512]{1,0:T(8,128)}), f32[32,512]{1,0:T(8,128)}) %reduce-scatter.14.cloned.1.call-update) | async-done | bytes 65552 | tf_op jit(solution)/shard_map/reduce_scatter | solution.py:73
  103.2 27.0 %reduce-scatter.8.cloned.1.call-done = f32[32,512]{1,0:T(8,128)} async-done(((f32[128,512]{1,0:T(8,128)}), f32[32,512]{1,0:T(8,128)}) %reduce-scatter.8.cloned.1.call-update) | async-done | bytes 65552 | tf_op jit(solution)/shard_map/reduce_scatter | solution.py:70
  131.5 8.2 %multiply_add_fusion = f32[32,4,128,128]{3,2,1,0:T(8,128)S(1)} fusion(f32[32,4,128,128]{3,2,1,0:T(8,128)} %param.21, f32[32,4,128]{2,1,0:T(4,128)S(1)} %mul.164, f32[32,4,128]{2,1,0:T(4,128)S(1)} %bitcast.37, f32[32,4,128]{2,1,0:T(4,128)S(1)} %bitcast.36), kind=kLoop, calls=%fused_computation | loop fusion | flops 6291456 | bytes 16973824 | tf_op jit(solution)/shard_map/add | solution.py:82
  139.8 7.2 %fusion.18 = f32[32,4,1,128]{3,2,1,0:T(1,128)S(1)} fusion(f32[32,4,128,1]{2,3,1,0:T(1,128)S(1)} %bitcast.35, f32[32,4,128,128]{3,2,1,0:T(8,128)S(1)} %multiply_add_fusion), kind=kOutput, calls=%fused_computation.39 | convolution fusion | flops 25165824 | bytes 8519680 | tf_op jit(solution)/shard_map/shc,shce->she/dot_general | solution.py:83
  147.3 8.5 %all_gather.13 = bf16[128,512]{1,0:T(8,128)(2,1)S(1)} all-gather(bf16[32,512]{1,0:T(8,128)(2,1)S(1)} %bitcast.40), channel_id=1, replica_groups=mesh['kv'=4,'tp'=8] {'kv'}, dimensions={0}, use_global_device_ids=true | all-gather | bytes 163840 | tf_op jit(solution)/shard_map/all_gather | solution.py:91
  157.0 56.6 %all-reduce.3.cloned.1.call-done = f32[128,1024]{1,0:T(8,128)} async-done(((f32[128,1024]{1,0:T(8,128)}), f32[128,1024]{1,0:T(8,128)}) %all-reduce.3.cloned.1.call-update) | async-done | bytes 524304 | tf_op jit(solution)/shard_map/psum | solution.py:92
  213.6 1.2 multiply_reduce_fusion
  214.8 1.6 convolution_convert_fusion
  216.5 3.4 %convolution_convert_fusion.1 = bf16[128,1344]{0,1:T(8,128)(2,1)} fusion(bf16[1024,1344]{0,1:T(8,128)(2,1)} %param.25, f32[128,1024]{1,0:T(8,128)S(1)} %get-tuple-element.3, f32[1024]{0:T(1024)S(1)} %copy-done.4), kind=kOutput, calls=%fused_computation.2 | convolution fusion | flops 352755712 | bytes 3624960 | tf_op jit(solution)/shard_map/dot_general | solution.py:24
  220.0 10.3 %psum.31 = f32[128]{0:T(128)S(1)} all-reduce(f32[128]{0:T(128)S(1)} %get-tuple-element.2), channel_id=1, replica_groups=mesh['kv'=4,'tp'=8] {'kv'}, use_global_device_ids=true, to_apply=%region_10.11 | all-reduce | flops 128 | bytes 1024 | tf_op jit(solution)/shard_map/psum | solution.py:26
  230.3 14.4 %all-gather.3.cloned.1.call-done = bf16[512,1344]{0,1:T(8,128)(2,1)} async-done(((bf16[128,1344]{0,1:T(8,128)(2,1)}), bf16[512,1344]{0,1:T(8,128)(2,1)}) %all-gather.3.cloned.1.call-update) | async-done | bytes 1376272 | tf_op jit(solution)/shard_map/all_gather | solution.py:19
  244.7 3.7 %reshape.65 = bf16[4,128,1344]{1,0,2:T(4,128)(2,1)} reshape(bf16[512,1344]{0,1:T(8,128)(2,1)} %all-gather.3.cloned.1.call-done) | data formatting | bytes 2752512 | tf_op jit(solution)/shard_map/all_gather | solution.py:19
  248.4 8.9 %reduce_sum.42 = bf16[128,1344]{0,1:T(8,128)(2,1)} reduce(bf16[4,128,1344]{1,0,2:T(4,128)(2,1)} %reshape.65, bf16[]{:T(256)} %constant.39.clone.1), dimensions={0}, to_apply=%region_11.12 | reduce | flops 516096 | bytes 1720322 | tf_op jit(solution)/shard_map/reduce_sum | solution.py:19
  257.3 34.2 %all-reduce.5.cloned.1.call-done = bf16[128,1344]{0,1:T(8,128)(2,1)} async-done(((bf16[128,1344]{0,1:T(8,128)(2,1)}), bf16[128,1344]{0,1:T(8,128)(2,1)}) %all-reduce.5.cloned.1.call-update) | async-done | bytes 344080 | tf_op jit(solution)/shard_map/psum | solution.py:28
  291.5 2.8 convolution_convert_fusion.2
  295.1 31.1 %reduce-scatter.16.cloned.1.call-done = bf16[128,128]{1,0:T(8,128)(2,1)} async-done(((bf16[1024,128]{1,0:T(8,128)(2,1)}), bf16[128,128]{1,0:T(8,128)(2,1)}) %reduce-scatter.16.cloned.1.call-update) | async-done | bytes 32784
  (52 shorter events, 5.7 us)
Async XLA Ops:
  7.2 207.6 %copy-start = (bf16[1024,1344]{0,1:T(8,128)(2,1)S(1)}, bf16[1024,1344]{0,1:T(8,128)(2,1)}, u32[]{:S(2)}) copy-start(bf16[1024,1344]{0,1:T(8,128)(2,1)} %param.26) | copy-start | bytes 8257540
  7.2 19.9 %copy-start.3 = (f32[1024]{0:T(1024)S(1)}, f32[1024]{0:T(1024)}, u32[]{:S(2)}) copy-start(f32[1024]{0:T(1024)} %param.15) | copy-start | bytes 12292
  7.2 41.8 %reduce-scatter.10.cloned.1.call-start = ((), (), s32[]{:S(2)}) async-start(), calls=%async_computation.6 | async-start | bytes 327680 | tf_op jit(solution)/shard_map/reduce_scatter | solution.py:71
  24.7 17.2 %copy-start.5 = (f32[512]{0:T(512)S(1)}, f32[512]{0:T(512)}, u32[]{:S(2)}) copy-start(f32[512]{0:T(512)} %param.20) | copy-start | bytes 6148
  24.7 51.4 %reduce-scatter.12.cloned.1.call-start = ((), (), s32[]{:S(2)}) async-start(), calls=%async_computation.7 | async-start | bytes 327680 | tf_op jit(solution)/shard_map/reduce_scatter | solution.py:72
  27.0 76.2 %reduce-scatter.14.cloned.1.call-start = ((), (), s32[]{:S(2)}) async-start(), calls=%async_computation.8 | async-start | bytes 327680 | tf_op jit(solution)/shard_map/reduce_scatter | solution.py:73
  29.3 100.9 %reduce-scatter.8.cloned.1.call-start = ((), (), s32[]{:S(2)}) async-start(), calls=%async_computation.5 | async-start | bytes 327680 | tf_op jit(solution)/shard_map/reduce_scatter | solution.py:70
  31.6 181.9 %all-reduce.3.cloned.1.call-start = ((), (), s32[]{:S(2)}) async-start(), calls=%async_computation.9 | async-start | bytes 1048576 | tf_op jit(solution)/shard_map/psum | solution.py:92
  139.7 7.3 %copy-start.1 = (f32[32,4,128,128]{3,2,1,0:T(8,128)}, f32[32,4,128,128]{3,2,1,0:T(8,128)S(1)}, u32[]{:S(2)}) copy-start(f32[32,4,128,128]{3,2,1,0:T(8,128)S(1)} %multiply_add_fusion) | copy-start | bytes 25165828
  139.7 7.4 %copy-start.6 = (f32[128]{0:T(128)S(1)}, f32[128]{0:T(128)}, u32[]{:S(2)}) copy-start(f32[128]{0:T(128)} %param.22) | copy-start | bytes 1540
  139.8 16.0 %copy-start.2 = (bf16[512,1024]{1,0:T(8,128)(2,1)S(1)}, bf16[512,1024]{1,0:T(8,128)(2,1)}, u32[]{:S(2)}) copy-start(bf16[512,1024]{1,0:T(8,128)(2,1)} %param.23) | copy-start | bytes 3145732
  147.0 67.7 %copy-start.4 = (f32[1024]{0:T(1024)S(1)}, f32[1024]{0:T(1024)}, u32[]{:S(2)}) copy-start(f32[1024]{0:T(1024)} %param.24) | copy-start | bytes 12292
  157.0 87.8 %all-gather.3.cloned.1.call-start = ((), (), s32[]{:S(2)}) async-start(), calls=%async_computation.11 | async-start | bytes 1720320 | tf_op jit(solution)/shard_map/all_gather | solution.py:19
  216.4 75.0 %all-reduce.5.cloned.1.call-start = ((), (), s32[]{:S(2)}) async-start(), calls=%async_computation.10 | async-start | bytes 688128 | tf_op jit(solution)/shard_map/psum | solution.py:28
  219.9 106.2 %reduce-scatter.16.cloned.1.call-start = ((), (), s32[]{:S(2)}) async-start(), calls=%async_computation.12 | async-start | bytes 294912
Sparse Core Ops, SparseCore 0:
  24.8 24.1 reduce-scatter.9
  51.7 24.3 reduce-scatter.11
  78.9 24.3 reduce-scatter.13
  105.8 24.3 reduce-scatter.7
  157.1 56.4 all-reduce.2
  216.6 28.1 all-gather.2
  247.7 43.7 all-reduce.4
  295.2 30.9 reduce-scatter.15
